TPU v7x, 32 devices: a whole 2x2x4 slice. The times are simulated.
32 devices in a mesh: grp: 2 (over x), ep: 16 (over z, y, core).
Axes of the slice: x: 2, y: 2, z: 4, core: 2. Of those that a mesh axis runs over, the one named last changes fastest.
Arguments:
- tokens: bfloat16 [2048, 2048], P(('grp', 'ep')), parts along dimension 0, may hold values from -6 to 6
- lengths: int32 [256], P(('grp', 'ep')), parts along dimension 0, may hold values from 1 to 8, 384 in all
- experts: int32 [2048, 2], P(('grp', 'ep')), parts along dimension 0, may hold values from 0 to 3, all different within a row; in each aligned block of 64 rows (0 to 63, 64 to 127, ...) at most 64 rows name the same one
- route_weights: float32 [2048, 2], P(('grp', 'ep')), parts along dimension 0, may hold values from 0.2 to 1
- gate_proj: bfloat16 [16, 2048, 1792], P('ep'), may hold values from -0.125 to 0.125
- up_proj: bfloat16 [16, 2048, 1792], P('ep'), may hold values from -0.125 to 0.125
- down_proj: bfloat16 [16, 1792, 2048], P('ep'), may hold values from -0.0625 to 0.0625
- norm_gain: float32 [2048], replicated, may hold values from 0.1 to 1.9
- norm_bias: float32 [2048], replicated, may hold values from -3 to 3
Outputs:
- mixed: bfloat16 [2048, 2048], P(('grp', 'ep')), parts along dimension 0
There are 2 independent parts, one for each index of `grp`. A program takes and returns all parts, laid end to end along the dimension named above; an argument that names none is the same for every part. Nothing has to cross between parts.
Inputs may be any that keep to these rules, and one draw needn't show every extreme that they name: Each row names 2 different experts; in the rows of one device (aligned blocks of 64 rows) no expert is named by more than 64 rows. Within each copy of the problem the 128 lengths sum to 384; the whole array, over all copies, sums to that times the number of copies.
All inputs are finite; a program needn't handle non-finite values. No bound on the sum of `lengths` on one device may be relied on, other than what follows from the above.
Results may differ from a plain program's by a relative error of at most 0.0021.
Values may be sent and summed in bfloat16 or wider, within the bound.
A program may use at most 128 MiB of HBM per device.

v0:
```python
import jax
import jax.numpy as jnp
from jax import lax
from jax.sharding import PartitionSpec as P

SPLIT = 4
TOP = 2
SPAN = 8
RESIDUAL_SCALE = 8.0**0.25
NORM_EPS = 1e-05


def layer_norm(values, norm_gain, norm_bias):
    center = values - jnp.mean(values, -1, keepdims=True)
    variance = jnp.mean(center * center, -1, keepdims=True)
    return center * lax.rsqrt(variance + NORM_EPS) * norm_gain + norm_bias


def expert_rows(picked, gate_proj, up_proj, down_proj):
    pre_gate = jnp.dot(picked, gate_proj[0], preferred_element_type=jnp.float32)
    pre_up = jnp.dot(picked, up_proj[0], preferred_element_type=jnp.float32)
    hidden = (jax.nn.silu(pre_gate) * pre_up).astype(jnp.bfloat16)
    return jnp.dot(hidden, down_proj[0], preferred_element_type=jnp.float32)


def local(
    tokens, lengths, experts, route_weights, gate_proj, up_proj, down_proj, norm_gain, norm_bias
):
    slot_count, width = tokens.shape
    axis_count = lax.axis_size("ep")
    capacity = 2 * slot_count * TOP * SPLIT // axis_count
    position = jnp.arange(slot_count, dtype=jnp.int32)
    alive_mask = position % SPAN < jnp.repeat(lengths, SPAN, total_repeat_length=slot_count)
    inputs = tokens.astype(jnp.float32)
    gathered = lax.all_gather(tokens, "ep", axis=0, tiled=True)
    all_experts, all_lengths = (
        lax.all_gather(experts, "ep", axis=0, tiled=True),
        lax.all_gather(lengths, "ep", axis=0, tiled=True),
    )
    all_weights = lax.all_gather(route_weights, "ep", axis=0, tiled=True)
    total_slots = gathered.shape[0]
    all_position = jnp.arange(total_slots, dtype=jnp.int32)
    all_alive = all_position % SPAN < jnp.repeat(all_lengths, SPAN, total_repeat_length=total_slots)
    own_expert = lax.axis_index("ep") // SPLIT
    hits = (all_experts == own_expert) & all_alive[:, None]
    chosen = hits.reshape(total_slots * TOP).astype(jnp.int32)
    order_rank = jnp.cumsum(chosen) - 1
    row_count = axis_count * capacity
    rows_index = jnp.arange(row_count, dtype=jnp.int32)
    picker = (order_rank[None, :] == rows_index[:, None]) & (chosen[None, :] == 1)
    flat_slot = jnp.repeat(all_position, TOP, total_repeat_length=total_slots * TOP)
    row_source = jnp.sum(jnp.where(picker, flat_slot[None, :], 0), axis=1)
    picked = jnp.take(gathered, row_source, axis=0)
    results = expert_rows(picked, gate_proj, up_proj, down_proj)
    rank_pairs = order_rank.reshape(total_slots, TOP)
    slot_row = jnp.sum(jnp.where(hits, rank_pairs, 0), axis=1)
    slot_weight = jnp.sum(jnp.where(hits, all_weights, 0.0), axis=1)
    spread_back = jnp.take(results, slot_row, axis=0) * slot_weight[:, None]
    branch = lax.psum_scatter(spread_back, "ep", scatter_dimension=0, tiled=True)
    normed = layer_norm(RESIDUAL_SCALE * inputs + branch, norm_gain, norm_bias)
    return jnp.where(alive_mask[:, None], normed, 0.0).astype(jnp.bfloat16)


def solution(mesh):
    in_specs = (
        P(("grp", "ep"), None),
        P(("grp", "ep")),
        P(("grp", "ep"), None),
        P(("grp", "ep"), None),
        P("ep", None, None),
        P("ep", None, None),
        P("ep", None, None),
        P(),
        P(),
    )
    out_specs = P(("grp", "ep"), None)
    return jax.shard_map(local, mesh=mesh, in_specs=in_specs, out_specs=out_specs, check_vma=False)
```

profile of v0, /device:TPU:0, one launch (start us, length us, event | category | flops | bytes accessed | tf_op | source)
XLA Modules:
  0.0 260.8 jit_solution(14044084314716863981)
XLA Ops:
  6.5 0.0 all-gather.4.cloned.1.call-start
  6.5 0.7 all-gather.4.cloned.1.call-update
  7.3 0.0 reduce-scatter.2.cloned.1.call-start
  7.3 23.6 %all-gather = s32[16,64,2]{1,2,0:T(2,128)S(1)} all-gather(s32[1,64,2]{1,2,0:T(2,128)} %bitcast.52), channel_id=1, replica_groups=mesh['grp'=2,'ep'=16] {'ep'}, dimensions={0}, use_global_device_ids=true | all-gather | bytes 8704 | tf_op jit(solution)/shard_map/all_gather | solution.py:37
  30.9 0.1 reshape.405
  31.0 1.2 dynamic-slice.18
  32.9 0.9 dynamic-update-slice.8
  33.8 7.1 %all-reduce = s32[128]{0:T(128)S(1)} all-reduce(s32[128]{0:T(128)S(1)} %dynamic-update-slice.8), channel_id=1, replica_groups=mesh['grp'=2,'ep'=16] {'ep'}, use_global_device_ids=true, to_apply=%add | all-reduce | flops 128 | bytes 1024
  40.9 0.8 add_add_fusion.1
  41.7 6.6 %gather_fusion = s32[1024]{0:T(1024)S(1)} fusion(s32[128]{0:T(128)S(1)} %all-reduce, s32[1024]{0:T(1024)S(1)} %broadcast_clamp_fusion.2), kind=kCustom, calls=%fused_computation | custom fusion | bytes 12288 | tf_op jit(solution)/shard_map/jit(_take)/gather | solution.py:43
  48.3 0.8 fusion.12
  49.0 0.2 copy.26
  49.3 0.3 reshape.357
  49.5 0.3 reduce-window.23
  49.8 0.1 slice.72
  49.9 0.5 reshape.354
  50.4 23.2 %all-gather.1 = f32[16,64,2]{1,2,0:T(2,128)S(1)} all-gather(f32[1,64,2]{1,2,0:T(2,128)} %bitcast.53), channel_id=1, replica_groups=mesh['grp'=2,'ep'=16] {'ep'}, dimensions={0}, use_global_device_ids=true | all-gather | bytes 8704 | tf_op jit(solution)/shard_map/all_gather | solution.py:40
  73.6 0.1 reshape.403
  73.7 0.3 copy.28
  73.9 0.4 eq.44
  74.3 0.1 slice_reduce_fusion
  74.4 0.1 broadcast.380
  74.5 0.1 reshape.356
  74.6 0.2 copy.27
  74.9 0.1 add_bitcast_fusion
  74.9 2.5 select_reduce_fusion
  77.5 0.0 all-gather.4.cloned.1.call-done
  77.5 11.7 %gather_fusion.1 = bf16[1024,2048]{1,0:T(8,128)(2,1)} fusion(bf16[1024,2048]{1,0:T(8,128)(2,1)} %all-gather.4.cloned.1.call-done, s32[1024]{0:T(1024)S(1)} %broadcast_clamp_fusion.1), kind=kCustom, calls=%fused_computation.1 | custom fusion | bytes 8392704 | tf_op jit(solution)/shard_map/jit(_take)/gather | solution.py:53
  89.3 13.9 %fusion.5 = f32[1024,1792]{1,0:T(8,128)} fusion(bf16[1,2048,1792]{2,1,0:T(8,128)(2,1)} %param.19, bf16[1024,2048]{1,0:T(8,128)(2,1)} %gather_fusion.1, pred[1024]{0:T(1024)(128)(4,1)S(1)} %compare_and_fusion), kind=kOutput, calls=%fused_computation.11 | convolution fusion | flops 7518289920 | bytes 18875392 | tf_op jit(solution)/shard_map/dot_general | solution.py:20
  103.1 26.9 %fusion.1 = f32[1024,2048]{1,0:T(8,128)} fusion(bf16[1,1792,2048]{2,1,0:T(8,128)(2,1)} %param.21, f32[1024,1792]{1,0:T(8,128)} %fusion.5, bf16[1,2048,1792]{2,1,0:T(8,128)(2,1)} %param.20, bf16[1024,2048]{1,0:T(8,128)(2,1)} %gather_fusion.1, pred[1024]{0:T(1024)(128)(4,1)S(1)} %compare_and_fusion), kind=kOutput, calls=%fused_computation.7 | convolution fusion | flops 15045492736 | bytes 34604032 | tf_op jit(solution)/shard_map/dot_general | solution.py:23
  130.1 12.5 %gather_fusion.2 = f32[1024,2048]{1,0:T(8,128)} fusion(f32[1024,2048]{1,0:T(8,128)} %fusion.1, s32[1024]{0:T(1024)S(1)} %broadcast_clamp_fusion), kind=kCustom, calls=%fused_computation.2 | custom fusion | bytes 16781312 | tf_op jit(solution)/shard_map/jit(_take)/gather | solution.py:58
  142.5 6.0 %select_multiply_fusion = f32[1024,2048]{1,0:T(8,128)} fusion(f32[1024,2048]{1,0:T(8,128)} %gather_fusion.2, f32[1024]{0:T(1024)S(1)} %select_reduce_fusion.1, pred[1024]{0:T(1024)(128)(4,1)S(1)} %compare_and_fusion.1), kind=kLoop, calls=%fused_computation.3 | loop fusion | flops 4194304 | bytes 16782336 | tf_op jit(solution)/shard_map/mul | solution.py:58
  148.5 0.0 copy-start.7
  148.5 0.0 copy-start.8
  148.5 0.0 copy-start.9
  148.5 0.0 copy-start.10
  148.6 0.0 copy-start
  148.6 0.0 copy-start.2
  148.6 0.0 copy-start.3
  148.6 0.0 reduce-scatter.2.cloned.1.call-update
  148.6 0.5 copy-done.1
  149.1 0.7 fusion.22
  149.8 0.0 copy-done.4
  149.9 5.1 %fusion.16 = pred[64]{0:T(512)(128)(4,1)S(1)} fusion(pred[64]{0:T(512)(128)(4,1)S(1)} %copy-done.10, pred[64]{0:T(512)(128)(4,1)S(1)} %copy-done.9, pred[64]{0:T(512)(128)(4,1)S(1)} %copy-done.8, pred[64]{0:T(512)(128)(4,1)S(1)} %copy-done.7, pred[64]{0:T(512)(128)(4,1)S(1)} %copy-done.6, pred[64]{0:T(512)(128)(4,1)S(1)} %copy-done.5, ...), kind=kLoop, calls=%fused_computation.46 | loop fusion | flops 896 | bytes 544 | tf_op jit(solution)/shard_map/lt | solution.py:33
  154.9 94.5 %reduce-scatter.2.cloned.1.call-done = f32[64,2048]{1,0:T(8,128)} async-done(((f32[1024,2048]{1,0:T(8,128)}), f32[64,2048]{1,0:T(8,128)}) %reduce-scatter.2.cloned.1.call-update) | async-done | bytes 524304 | tf_op jit(solution)/shard_map/reduce_scatter | solution.py:59
  249.5 1.2 fusion.11
  250.7 1.3 multiply_reduce_fusion
  252.0 1.9 select_convert_fusion
  (31 shorter events, 0.2 us)
Async XLA Ops:
  6.5 71.0 %all-gather.4.cloned.1.call-start = ((), (), s32[]{:S(2)}) async-start(), calls=%async_computation.1 | async-start | bytes 4456448 | tf_op jit(solution)/shard_map/all_gather | solution.py:35
  7.3 242.2 %reduce-scatter.2.cloned.1.call-start = ((), (), s32[]{:S(2)}) async-start(), calls=%async_computation.2 | async-start | bytes 8912896 | tf_op jit(solution)/shard_map/reduce_scatter | solution.py:59
  148.5 0.7 copy-start.1
  148.5 1.3 copy-start.4
  148.5 1.3 copy-start.5
  148.5 1.3 copy-start.6
  148.5 1.3 copy-start.7
  148.5 1.3 copy-start.8
  148.5 1.3 copy-start.9
  148.5 1.3 copy-start.10
  148.6 100.9 %copy-start = (bf16[64,2048]{1,0:T(8,128)(2,1)S(1)}, bf16[64,2048]{1,0:T(8,128)(2,1)}, u32[]{:S(2)}) copy-start(bf16[64,2048]{1,0:T(8,128)(2,1)} %param.15) | copy-start | bytes 786436
  148.6 103.4 %copy-start.2 = (f32[2048]{0:T(1024)S(1)}, f32[2048]{0:T(1024)}, u32[]{:S(2)}) copy-start(f32[2048]{0:T(1024)} %param.23) | copy-start | bytes 24580
  148.6 103.4 %copy-start.3 = (f32[2048]{0:T(1024)S(1)}, f32[2048]{0:T(1024)}, u32[]{:S(2)}) copy-start(f32[2048]{0:T(1024)} %param.22) | copy-start | bytes 24580
Sparse Core Ops, SparseCore 0:
  9.5 53.3 all-gather.3
  148.7 100.6 reduce-scatter.1
where the time goes:
time: 261 us
  waiting for transfers between devices  95.3 us (37%)
  blocking collectives  53.9 us (21%)
  matrix products  40.8 us (16%)
  local copies, waits for them, and re-layouts  36.4 us (14%)
  other arithmetic  20 us (8%)
  between operations  14.3 us (5%)
    reduce_scatter x1, waiting for transfers between devices, local(): lax.psum_scatter(spread_back, 'ep', scatter_dimension=0, tiled=True)  94.5 us
    dot_general x1, matrix products, expert_rows(): return jnp.dot(hidden, down_proj[0], preferred_element_type=jnp.float32)  26.9 us
    all_gather x1, blocking collectives, local(): lax.all_gather(experts, 'ep', axis=0, tiled=True)  23.6 us
    all_gather x1, blocking collectives, local(): all_weights = lax.all_gather(route_weights, 'ep', axis=0, tiled=True)  23.2 us
    dot_general x1, matrix products, expert_rows(): pre_gate = jnp.dot(picked, gate_proj[0], preferred_element_type=jnp.float32)  13.9 us
    gather x1, local copies, waits for them, and re-layouts, local(): spread_back = jnp.take(results, slot_row, axis=0) * slot_weight[:, None]  12.5 us
    gather x1, local copies, waits for them, and re-layouts, local(): picked = jnp.take(gathered, row_source, axis=0)  11.7 us
    unnamed x1, blocking collectives  7.11 us
  transfers between devices with their start and end apart: 2, of which 1 were waited for; matrix products, arithmetic and copies ran while one was open for 8% of the time, Pallas kernels for 0%

commit v1 on v0

--- a/solution.py
+++ b/solution.py
@@ -8,6 +8,16 @@
 SPAN = 8
 RESIDUAL_SCALE = 8.0**0.25
 NORM_EPS = 1e-05
+
+
+def gather_by_hops(x, mesh_axis, dim):
+    n_dev = lax.axis_size(mesh_axis)
+    held, blocks = (x, [x])
+    for _ in range(n_dev - 1):
+        held = lax.ppermute(held, mesh_axis, [(i, (i + 1) % n_dev) for i in range(n_dev)])
+        blocks.insert(0, held)
+    merged = jnp.concatenate(blocks, axis=dim)
+    return jnp.roll(merged, (lax.axis_index(mesh_axis) + 1) * x.shape[dim], axis=dim)
 
 
 def layer_norm(values, norm_gain, norm_bias):
@@ -37,7 +47,7 @@
         lax.all_gather(experts, "ep", axis=0, tiled=True),
         lax.all_gather(lengths, "ep", axis=0, tiled=True),
     )
-    all_weights = lax.all_gather(route_weights, "ep", axis=0, tiled=True)
+    all_weights = gather_by_hops(route_weights, "ep", 0)
     total_slots = gathered.shape[0]
     all_position = jnp.arange(total_slots, dtype=jnp.int32)
     all_alive = all_position % SPAN < jnp.repeat(all_lengths, SPAN, total_repeat_length=total_slots)

time: 261 us -> 313 us (1.20)
  waiting for transfers between devices: 95.3 us -> 169 us
  blocking collectives: 53.9 us -> 30.2 us
    ppermute x0 -> x15, waiting for transfers between devices: none -> 73.9 us  [gather_by_hops(): lax.ppermute(held, mesh_axis, [(i, (i + 1) % n_dev) for i in range(n_dev)])]
    all_gather x1 -> x0, blocking collectives: 23.2 us -> none  [local(): all_weights = lax.all_gather(route_weights, 'ep', axis=0, tiled=True)]
  transfers between devices with their start and end apart: 2 -> 17, of which waited for: 1 -> 15; matrix products, arithmetic and copies ran while one was open for 8% -> 7% of each run, Pallas kernels for 0% -> 0%
where the time goes in v1:
time: 313 us; the launch traced here: 312 us
  waiting for transfers between devices  169 us (54%)
  matrix products  40.8 us (13%)
  local copies, waits for them, and re-layouts  37.1 us (12%)
  blocking collectives  30.2 us (10%)
  other arithmetic  19.9 us (6%)
  between operations  14.3 us (5%)
    reduce_scatter x1, waiting for transfers between devices, local(): lax.psum_scatter(spread_back, 'ep', scatter_dimension=0, tiled=True)  94.6 us
    ppermute x15, waiting for transfers between devices, gather_by_hops(): lax.ppermute(held, mesh_axis, [(i, (i + 1) % n_dev) for i in range(n_dev)])  73.9 us
    dot_general x1, matrix products, expert_rows(): return jnp.dot(hidden, down_proj[0], preferred_element_type=jnp.float32)  26.9 us
    all_gather x1, blocking collectives, local(): lax.all_gather(experts, 'ep', axis=0, tiled=True)  23 us
    dot_general x1, matrix products, expert_rows(): pre_gate = jnp.dot(picked, gate_proj[0], preferred_element_type=jnp.float32)  13.9 us
    gather x1, local copies, waits for them, and re-layouts, local(): spread_back = jnp.take(results, slot_row, axis=0) * slot_weight[:, None]  12.4 us
    gather x1, local copies, waits for them, and re-layouts, local(): picked = jnp.take(gathered, row_source, axis=0)  11.7 us
    unnamed x1, blocking collectives  7.26 us
  transfers between devices with their start and end apart: 17, of which 15 were waited for; matrix products, arithmetic and copies ran while one was open for 7% of the time, Pallas kernels for 0%

profile of v1, /device:TPU:0, one launch (start us, length us, event | category | flops | bytes accessed | tf_op | source)
XLA Modules:
  0.0 312.3 jit_solution(15416777731591066100)
XLA Ops:
  6.5 0.7 all-gather.3.cloned.1.call-update
  7.3 0.5 collective-permute-start
  7.8 1.2 dynamic-slice.18
  9.7 23.0 %all-gather = s32[16,64,2]{1,2,0:T(2,128)S(1)} all-gather(s32[1,64,2]{1,2,0:T(2,128)} %bitcast.49), channel_id=1, replica_groups=mesh['grp'=2,'ep'=16] {'ep'}, dimensions={0}, use_global_device_ids=true | all-gather | bytes 8704 | tf_op jit(solution)/shard_map/all_gather | solution.py:47
  32.7 0.8 add_add_fusion.1
  33.5 0.9 dynamic-update-slice.8
  34.4 7.3 %all-reduce = s32[128]{0:T(128)S(1)} all-reduce(s32[128]{0:T(128)S(1)} %dynamic-update-slice.8), channel_id=1, replica_groups=mesh['grp'=2,'ep'=16] {'ep'}, use_global_device_ids=true, to_apply=%add | all-reduce | flops 128 | bytes 1024
  41.6 6.6 %gather_fusion = s32[1024]{0:T(1024)S(1)} fusion(s32[128]{0:T(128)S(1)} %all-reduce, s32[1024]{0:T(1024)S(1)} %broadcast_clamp_fusion.2), kind=kCustom, calls=%fused_computation | custom fusion | bytes 12288 | tf_op jit(solution)/shard_map/jit(_take)/gather | solution.py:53
  48.3 0.8 fusion.12
  49.0 0.1 reshape.403
  49.1 4.8 %collective-permute-done.1 = f32[64,2]{0,1:T(2,128)S(1)} collective-permute-done((f32[64,2]{0,1:T(2,128)S(1)}, f32[64,2]{0,1:T(2,128)S(1)}, u32[]{:S(2)}, u32[]{:S(2)}) %collective-permute-start.1) | collective-permute-done | bytes 544 | tf_op jit(solution)/shard_map/ppermute | solution.py:17
  54.0 0.2 copy.24
  54.2 0.3 reshape.357
  54.5 0.3 reduce-window.23
  54.8 0.1 slice.72
  54.9 4.9 %collective-permute-done.2 = f32[64,2]{0,1:T(2,128)S(1)} collective-permute-done((f32[64,2]{0,1:T(2,128)S(1)}, f32[64,2]{0,1:T(2,128)S(1)}, u32[]{:S(2)}, u32[]{:S(2)}) %collective-permute-start.2) | collective-permute-done | bytes 544 | tf_op jit(solution)/shard_map/ppermute | solution.py:17
  59.8 0.1 slice_reduce_fusion
  59.9 5.6 %collective-permute-done.3 = f32[64,2]{0,1:T(2,128)S(1)} collective-permute-done((f32[64,2]{0,1:T(2,128)S(1)}, f32[64,2]{0,1:T(2,128)S(1)}, u32[]{:S(2)}, u32[]{:S(2)}) %collective-permute-start.3) | collective-permute-done | bytes 544 | tf_op jit(solution)/shard_map/ppermute | solution.py:17
  65.6 0.3 copy.26
  65.9 0.4 eq.47
  66.2 5.0 %collective-permute-done.4 = f32[64,2]{0,1:T(2,128)S(1)} collective-permute-done((f32[64,2]{0,1:T(2,128)S(1)}, f32[64,2]{0,1:T(2,128)S(1)}, u32[]{:S(2)}, u32[]{:S(2)}) %collective-permute-start.4) | collective-permute-done | bytes 544 | tf_op jit(solution)/shard_map/ppermute | solution.py:17
  71.2 2.5 select_reduce_fusion
  73.7 3.2 %collective-permute-done.5 = f32[64,2]{0,1:T(2,128)S(1)} collective-permute-done((f32[64,2]{0,1:T(2,128)S(1)}, f32[64,2]{0,1:T(2,128)S(1)}, u32[]{:S(2)}, u32[]{:S(2)}) %collective-permute-start.5) | collective-permute-done | bytes 544 | tf_op jit(solution)/shard_map/ppermute | solution.py:17
  76.9 5.7 %collective-permute-done.6 = f32[64,2]{0,1:T(2,128)S(1)} collective-permute-done((f32[64,2]{0,1:T(2,128)S(1)}, f32[64,2]{0,1:T(2,128)S(1)}, u32[]{:S(2)}, u32[]{:S(2)}) %collective-permute-start.6) | collective-permute-done | bytes 544 | tf_op jit(solution)/shard_map/ppermute | solution.py:17
  82.6 0.5 reshape.354
  83.2 0.2 copy.25
  83.4 4.9 %collective-permute-done.7 = f32[64,2]{0,1:T(2,128)S(1)} collective-permute-done((f32[64,2]{0,1:T(2,128)S(1)}, f32[64,2]{0,1:T(2,128)S(1)}, u32[]{:S(2)}, u32[]{:S(2)}) %collective-permute-start.7) | collective-permute-done | bytes 544 | tf_op jit(solution)/shard_map/ppermute | solution.py:17
  88.3 5.7 %collective-permute-done.8 = f32[64,2]{0,1:T(2,128)S(1)} collective-permute-done((f32[64,2]{0,1:T(2,128)S(1)}, f32[64,2]{0,1:T(2,128)S(1)}, u32[]{:S(2)}, u32[]{:S(2)}) %collective-permute-start.8) | collective-permute-done | bytes 544 | tf_op jit(solution)/shard_map/ppermute | solution.py:17
  94.0 5.7 %collective-permute-done.9 = f32[64,2]{0,1:T(2,128)S(1)} collective-permute-done((f32[64,2]{0,1:T(2,128)S(1)}, f32[64,2]{0,1:T(2,128)S(1)}, u32[]{:S(2)}, u32[]{:S(2)}) %collective-permute-start.9) | collective-permute-done | bytes 544 | tf_op jit(solution)/shard_map/ppermute | solution.py:17
  99.7 5.7 %collective-permute-done.10 = f32[64,2]{0,1:T(2,128)S(1)} collective-permute-done((f32[64,2]{0,1:T(2,128)S(1)}, f32[64,2]{0,1:T(2,128)S(1)}, u32[]{:S(2)}, u32[]{:S(2)}) %collective-permute-start.10) | collective-permute-done | bytes 544 | tf_op jit(solution)/shard_map/ppermute | solution.py:17
  105.4 5.7 %collective-permute-done.11 = f32[64,2]{0,1:T(2,128)S(1)} collective-permute-done((f32[64,2]{0,1:T(2,128)S(1)}, f32[64,2]{0,1:T(2,128)S(1)}, u32[]{:S(2)}, u32[]{:S(2)}) %collective-permute-start.11) | collective-permute-done | bytes 544 | tf_op jit(solution)/shard_map/ppermute | solution.py:17
  111.1 5.7 %collective-permute-done.12 = f32[64,2]{0,1:T(2,128)S(1)} collective-permute-done((f32[64,2]{0,1:T(2,128)S(1)}, f32[64,2]{0,1:T(2,128)S(1)}, u32[]{:S(2)}, u32[]{:S(2)}) %collective-permute-start.12) | collective-permute-done | bytes 544 | tf_op jit(solution)/shard_map/ppermute | solution.py:17
  116.8 5.7 %collective-permute-done.13 = f32[64,2]{0,1:T(2,128)S(1)} collective-permute-done((f32[64,2]{0,1:T(2,128)S(1)}, f32[64,2]{0,1:T(2,128)S(1)}, u32[]{:S(2)}, u32[]{:S(2)}) %collective-permute-start.13) | collective-permute-done | bytes 544 | tf_op jit(solution)/shard_map/ppermute | solution.py:17
  122.5 5.7 %collective-permute-done.14 = f32[64,2]{0,1:T(2,128)S(1)} collective-permute-done((f32[64,2]{0,1:T(2,128)S(1)}, f32[64,2]{0,1:T(2,128)S(1)}, u32[]{:S(2)}, u32[]{:S(2)}) %collective-permute-start.14) | collective-permute-done | bytes 544 | tf_op jit(solution)/shard_map/ppermute | solution.py:17
  128.2 0.9 concatenate.18
  129.0 0.1 select_reduce_fusion.1
  129.2 11.7 %gather_fusion.1 = bf16[1024,2048]{1,0:T(8,128)(2,1)} fusion(bf16[1024,2048]{1,0:T(8,128)(2,1)} %all-gather.3.cloned.1.call-done, s32[1024]{0:T(1024)S(1)} %broadcast_clamp_fusion.1), kind=kCustom, calls=%fused_computation.1 | custom fusion | bytes 8392704 | tf_op jit(solution)/shard_map/jit(_take)/gather | solution.py:63
  140.9 13.9 %fusion.5 = f32[1024,1792]{1,0:T(8,128)} fusion(bf16[1,2048,1792]{2,1,0:T(8,128)(2,1)} %param.19, bf16[1024,2048]{1,0:T(8,128)(2,1)} %gather_fusion.1, pred[1024]{0:T(1024)(128)(4,1)S(1)} %compare_and_fusion), kind=kOutput, calls=%fused_computation.11 | convolution fusion | flops 7518289920 | bytes 18875392 | tf_op jit(solution)/shard_map/dot_general | solution.py:30
  154.8 26.9 %fusion.1 = f32[1024,2048]{1,0:T(8,128)} fusion(bf16[1,1792,2048]{2,1,0:T(8,128)(2,1)} %param.21, f32[1024,1792]{1,0:T(8,128)} %fusion.5, bf16[1,2048,1792]{2,1,0:T(8,128)(2,1)} %param.20, bf16[1024,2048]{1,0:T(8,128)(2,1)} %gather_fusion.1, pred[1024]{0:T(1024)(128)(4,1)S(1)} %compare_and_fusion), kind=kOutput, calls=%fused_computation.7 | convolution fusion | flops 15045492736 | bytes 34604032 | tf_op jit(solution)/shard_map/dot_general | solution.py:33
  181.7 12.4 %gather_fusion.2 = f32[1024,2048]{1,0:T(8,128)} fusion(f32[1024,2048]{1,0:T(8,128)} %fusion.1, s32[1024]{0:T(1024)S(1)} %broadcast_clamp_fusion), kind=kCustom, calls=%fused_computation.2 | custom fusion | bytes 16781312 | tf_op jit(solution)/shard_map/jit(_take)/gather | solution.py:68
  194.1 6.0 %select_multiply_fusion = f32[1024,2048]{1,0:T(8,128)} fusion(f32[1024,2048]{1,0:T(8,128)} %gather_fusion.2, f32[1024]{0:T(1024)S(1)} %select_reduce_fusion.1, pred[1024]{0:T(1024)(128)(4,1)S(1)} %compare_and_fusion.1), kind=kLoop, calls=%fused_computation.3 | loop fusion | flops 4194304 | bytes 16782336 | tf_op jit(solution)/shard_map/mul | solution.py:68
  200.2 0.5 copy-done.1
  200.7 0.7 fusion.22
  201.4 5.0 %fusion.16 = pred[64]{0:T(512)(128)(4,1)S(1)} fusion(pred[64]{0:T(512)(128)(4,1)S(1)} %copy-done.10, pred[64]{0:T(512)(128)(4,1)S(1)} %copy-done.9, pred[64]{0:T(512)(128)(4,1)S(1)} %copy-done.8, pred[64]{0:T(512)(128)(4,1)S(1)} %copy-done.7, pred[64]{0:T(512)(128)(4,1)S(1)} %copy-done.6, pred[64]{0:T(512)(128)(4,1)S(1)} %copy-done.5, ...), kind=kLoop, calls=%fused_computation.46 | loop fusion | flops 896 | bytes 544 | tf_op jit(solution)/shard_map/lt | solution.py:43
  206.4 94.6 %reduce-scatter.2.cloned.1.call-done = f32[64,2048]{1,0:T(8,128)} async-done(((f32[1024,2048]{1,0:T(8,128)}), f32[64,2048]{1,0:T(8,128)}) %reduce-scatter.2.cloned.1.call-update) | async-done | bytes 524304 | tf_op jit(solution)/shard_map/reduce_scatter | solution.py:69
  301.0 1.2 fusion.11
  302.3 1.3 multiply_reduce_fusion
  303.6 1.9 select_convert_fusion
  (59 shorter events, 0.6 us)
Async XLA Ops:
  6.5 122.6 %all-gather.3.cloned.1.call-start = ((), (), s32[]{:S(2)}) async-start(), calls=%async_computation.1 | async-start | bytes 4456448 | tf_op jit(solution)/shard_map/all_gather | solution.py:45
  7.3 293.8 %reduce-scatter.2.cloned.1.call-start = ((), (), s32[]{:S(2)}) async-start(), calls=%async_computation.2 | async-start | bytes 8912896 | tf_op jit(solution)/shard_map/reduce_scatter | solution.py:69
  7.3 40.9 %collective-permute-start = (f32[64,2]{0,1:T(2,128)}, f32[64,2]{0,1:T(2,128)S(1)}, u32[]{:S(2)}, u32[]{:S(2)}) collective-permute-start(f32[64,2]{0,1:T(2,128)} %param.18), channel_id=1, source_target_pairs={{0,1},{1,2},{2,3},{3,4},{4,5},{5,6},{6,7},{7,8},{8,9},{9,10},{10,1... | collective-permute-start | bytes 1544 | tf_op jit(solution)/shard_map/ppermute | solution.py:17
  48.2 5.7 %collective-permute-start.1 = (f32[64,2]{0,1:T(2,128)S(1)}, f32[64,2]{0,1:T(2,128)S(1)}, u32[]{:S(2)}, u32[]{:S(2)}) collective-permute-start(f32[64,2]{0,1:T(2,128)S(1)} %collective-permute-done), channel_id=1, source_target_pairs={{0,1},{1,2},{2,3},{3,4},{4,5},{5,6},{6,7},{7,8},{8,9},{9,10},{10,1... | collective-permute-start | bytes 1544 | tf_op jit(solution)/shard_map/ppermute | solution.py:17
  54.0 5.8 %collective-permute-start.2 = (f32[64,2]{0,1:T(2,128)S(1)}, f32[64,2]{0,1:T(2,128)S(1)}, u32[]{:S(2)}, u32[]{:S(2)}) collective-permute-start(f32[64,2]{0,1:T(2,128)S(1)} %collective-permute-done.1), channel_id=1, source_target_pairs={{0,1},{1,2},{2,3},{3,4},{4,5},{5,6},{6,7},{7,8},{8,9},{9,10},{10,1... | collective-permute-start | bytes 1544 | tf_op jit(solution)/shard_map/ppermute | solution.py:17
  59.8 5.7 %collective-permute-start.3 = (f32[64,2]{0,1:T(2,128)S(1)}, f32[64,2]{0,1:T(2,128)S(1)}, u32[]{:S(2)}, u32[]{:S(2)}) collective-permute-start(f32[64,2]{0,1:T(2,128)S(1)} %collective-permute-done.2), channel_id=1, source_target_pairs={{0,1},{1,2},{2,3},{3,4},{4,5},{5,6},{6,7},{7,8},{8,9},{9,10},{10,1... | collective-permute-start | bytes 1544 | tf_op jit(solution)/shard_map/ppermute | solution.py:17
  65.5 5.7 %collective-permute-start.4 = (f32[64,2]{0,1:T(2,128)S(1)}, f32[64,2]{0,1:T(2,128)S(1)}, u32[]{:S(2)}, u32[]{:S(2)}) collective-permute-start(f32[64,2]{0,1:T(2,128)S(1)} %collective-permute-done.3), channel_id=1, source_target_pairs={{0,1},{1,2},{2,3},{3,4},{4,5},{5,6},{6,7},{7,8},{8,9},{9,10},{10,1... | collective-permute-start | bytes 1544 | tf_op jit(solution)/shard_map/ppermute | solution.py:17
  71.2 5.7 %collective-permute-start.5 = (f32[64,2]{0,1:T(2,128)S(1)}, f32[64,2]{0,1:T(2,128)S(1)}, u32[]{:S(2)}, u32[]{:S(2)}) collective-permute-start(f32[64,2]{0,1:T(2,128)S(1)} %collective-permute-done.4), channel_id=1, source_target_pairs={{0,1},{1,2},{2,3},{3,4},{4,5},{5,6},{6,7},{7,8},{8,9},{9,10},{10,1... | collective-permute-start | bytes 1544 | tf_op jit(solution)/shard_map/ppermute | solution.py:17
  76.9 5.7 %collective-permute-start.6 = (f32[64,2]{0,1:T(2,128)S(1)}, f32[64,2]{0,1:T(2,128)S(1)}, u32[]{:S(2)}, u32[]{:S(2)}) collective-permute-start(f32[64,2]{0,1:T(2,128)S(1)} %collective-permute-done.5), channel_id=1, source_target_pairs={{0,1},{1,2},{2,3},{3,4},{4,5},{5,6},{6,7},{7,8},{8,9},{9,10},{10,1... | collective-permute-start | bytes 1544 | tf_op jit(solution)/shard_map/ppermute | solution.py:17
  82.6 5.7 %collective-permute-start.7 = (f32[64,2]{0,1:T(2,128)S(1)}, f32[64,2]{0,1:T(2,128)S(1)}, u32[]{:S(2)}, u32[]{:S(2)}) collective-permute-start(f32[64,2]{0,1:T(2,128)S(1)} %collective-permute-done.6), channel_id=1, source_target_pairs={{0,1},{1,2},{2,3},{3,4},{4,5},{5,6},{6,7},{7,8},{8,9},{9,10},{10,1... | collective-permute-start | bytes 1544 | tf_op jit(solution)/shard_map/ppermute | solution.py:17
  88.3 5.7 %collective-permute-start.8 = (f32[64,2]{0,1:T(2,128)S(1)}, f32[64,2]{0,1:T(2,128)S(1)}, u32[]{:S(2)}, u32[]{:S(2)}) collective-permute-start(f32[64,2]{0,1:T(2,128)S(1)} %collective-permute-done.7), channel_id=1, source_target_pairs={{0,1},{1,2},{2,3},{3,4},{4,5},{5,6},{6,7},{7,8},{8,9},{9,10},{10,1... | collective-permute-start | bytes 1544 | tf_op jit(solution)/shard_map/ppermute | solution.py:17
  94.0 5.7 %collective-permute-start.9 = (f32[64,2]{0,1:T(2,128)S(1)}, f32[64,2]{0,1:T(2,128)S(1)}, u32[]{:S(2)}, u32[]{:S(2)}) collective-permute-start(f32[64,2]{0,1:T(2,128)S(1)} %collective-permute-done.8), channel_id=1, source_target_pairs={{0,1},{1,2},{2,3},{3,4},{4,5},{5,6},{6,7},{7,8},{8,9},{9,10},{10,1... | collective-permute-start | bytes 1544 | tf_op jit(solution)/shard_map/ppermute | solution.py:17
  99.7 5.7 %collective-permute-start.10 = (f32[64,2]{0,1:T(2,128)S(1)}, f32[64,2]{0,1:T(2,128)S(1)}, u32[]{:S(2)}, u32[]{:S(2)}) collective-permute-start(f32[64,2]{0,1:T(2,128)S(1)} %collective-permute-done.9), channel_id=1, source_target_pairs={{0,1},{1,2},{2,3},{3,4},{4,5},{5,6},{6,7},{7,8},{8,9},{9,10},{10,1... | collective-permute-start | bytes 1544 | tf_op jit(solution)/shard_map/ppermute | solution.py:17
  105.4 5.7 %collective-permute-start.11 = (f32[64,2]{0,1:T(2,128)S(1)}, f32[64,2]{0,1:T(2,128)S(1)}, u32[]{:S(2)}, u32[]{:S(2)}) collective-permute-start(f32[64,2]{0,1:T(2,128)S(1)} %collective-permute-done.10), channel_id=1, source_target_pairs={{0,1},{1,2},{2,3},{3,4},{4,5},{5,6},{6,7},{7,8},{8,9},{9,10},{10,1... | collective-permute-start | bytes 1544 | tf_op jit(solution)/shard_map/ppermute | solution.py:17
  111.1 5.7 %collective-permute-start.12 = (f32[64,2]{0,1:T(2,128)S(1)}, f32[64,2]{0,1:T(2,128)S(1)}, u32[]{:S(2)}, u32[]{:S(2)}) collective-permute-start(f32[64,2]{0,1:T(2,128)S(1)} %collective-permute-done.11), channel_id=1, source_target_pairs={{0,1},{1,2},{2,3},{3,4},{4,5},{5,6},{6,7},{7,8},{8,9},{9,10},{10,1... | collective-permute-start | bytes 1544 | tf_op jit(solution)/shard_map/ppermute | solution.py:17
  116.8 5.7 %collective-permute-start.13 = (f32[64,2]{0,1:T(2,128)S(1)}, f32[64,2]{0,1:T(2,128)S(1)}, u32[]{:S(2)}, u32[]{:S(2)}) collective-permute-start(f32[64,2]{0,1:T(2,128)S(1)} %collective-permute-done.12), channel_id=1, source_target_pairs={{0,1},{1,2},{2,3},{3,4},{4,5},{5,6},{6,7},{7,8},{8,9},{9,10},{10,1... | collective-permute-start | bytes 1544 | tf_op jit(solution)/shard_map/ppermute | solution.py:17
  122.5 5.7 %collective-permute-start.14 = (f32[64,2]{0,1:T(2,128)S(1)}, f32[64,2]{0,1:T(2,128)S(1)}, u32[]{:S(2)}, u32[]{:S(2)}) collective-permute-start(f32[64,2]{0,1:T(2,128)S(1)} %collective-permute-done.13), channel_id=1, source_target_pairs={{0,1},{1,2},{2,3},{3,4},{4,5},{5,6},{6,7},{7,8},{8,9},{9,10},{10,1... | collective-permute-start | bytes 1544 | tf_op jit(solution)/shard_map/ppermute | solution.py:17
  200.0 0.7 copy-start.1
  200.1 1.3 copy-start.4
  200.1 1.3 copy-start.5
  200.1 1.3 copy-start.6
  200.1 1.3 copy-start.7
  200.1 1.3 copy-start.8
  200.1 1.3 copy-start.9
  200.1 1.3 copy-start.10
  200.1 100.9 %copy-start = (bf16[64,2048]{1,0:T(8,128)(2,1)S(1)}, bf16[64,2048]{1,0:T(8,128)(2,1)}, u32[]{:S(2)}) copy-start(bf16[64,2048]{1,0:T(8,128)(2,1)} %param.15) | copy-start | bytes 786436
  200.1 103.4 %copy-start.2 = (f32[2048]{0:T(1024)S(1)}, f32[2048]{0:T(1024)}, u32[]{:S(2)}) copy-start(f32[2048]{0:T(1024)} %param.23) | copy-start | bytes 24580
  200.1 103.4 %copy-start.3 = (f32[2048]{0:T(1024)S(1)}, f32[2048]{0:T(1024)}, u32[]{:S(2)}) copy-start(f32[2048]{0:T(1024)} %param.22) | copy-start | bytes 24580
Sparse Core Ops, SparseCore 0:
  9.5 53.2 all-gather.2
  200.3 100.6 reduce-scatter.1
